TPU v7x, 32 devices: a whole 2x2x4 slice. The times are simulated.
32 devices in a mesh: sp: 16 (over z, y, x), tp: 2 (over core).
Axes of the slice: x: 2, y: 2, z: 4, core: 2. Of those that a mesh axis runs over, the one named last changes fastest.
Arguments:
- tokens: bfloat16 [4096, 2048], P('sp', 'tp'), may hold values from -24 to 24
- value_weight: bfloat16 [2, 2048, 2048], P(None, 'sp', 'tp'), may hold values from -0.125 to 0.125
- outer_weight: bfloat16 [2, 2048, 2048], P(None, 'sp', 'tp'), may hold values from -0.125 to 0.125
- inner_weight: bfloat16 [2, 2048, 2048], P(None, 'sp', 'tp'), may hold values from -0.125 to 0.125
- conv_taps: float32 [2, 3, 2048], P(None, None, 'tp'), may hold values from -3.5 to 3.5
- output_weight: bfloat16 [2, 2048, 2048], P(None, 'tp', 'sp'), may hold values from -2 to 2
- norm_gain: float32 [2, 2048], P(None, 'tp'), may hold values from 0.1 to 1.9
- norm_bias: float32 [2, 2048], P(None, 'tp'), may hold values from -3 to 3
Outputs:
- mixed_out: bfloat16 [4096, 2048], P('sp', 'tp')
All inputs are finite; a program needn't handle non-finite values.
Results may differ from a plain program's by a relative error of at most 0.03.
Values may be sent and summed in bfloat16 or wider, within the bound.
A program may use at most 64 MiB of HBM per device.

v0:
```python
import jax
import jax.numpy as jnp
from jax import lax
from jax.sharding import PartitionSpec as P

D = 2048
LAYERS = 2


def from_behind(array, axis, by):
    peers = lax.axis_size(axis)
    pairs = [(i, i + by) for i in range(peers) if 0 <= i + by < peers]
    return lax.ppermute(array, axis, pairs)


def input_products(whole, weights):
    return tuple(
        (
            jnp.dot(whole, weight, preferred_element_type=jnp.float32).astype(jnp.bfloat16)
            for weight in weights
        )
    )


def shards(
    tokens, value_weight, outer_weight, inner_weight, conv_taps, output_weight, norm_gain, norm_bias
):
    alpha = (2.0 * LAYERS) ** 0.25
    state = tokens
    taps_count = conv_taps.shape[1]
    all_value, all_outer, all_inner, all_output = (
        lax.all_gather(value_weight, "sp", axis=1, tiled=True),
        lax.all_gather(outer_weight, "sp", axis=1, tiled=True),
        lax.all_gather(inner_weight, "sp", axis=1, tiled=True),
        lax.all_gather(output_weight, "sp", axis=2, tiled=True),
    )
    for layer in range(LAYERS):
        whole = lax.all_gather(state, "tp", axis=1, tiled=True)
        u_part, outer, inner = input_products(
            whole, (all_value[layer], all_outer[layer], all_inner[layer])
        )
        gated_in = inner.astype(jnp.float32) * u_part.astype(jnp.float32)
        previous = from_behind(gated_in[gated_in.shape[0] - (taps_count - 1) :], "sp", 1)
        padded = jnp.concatenate([previous, gated_in], axis=0)
        conv = jnp.zeros_like(gated_in)
        for tap in range(taps_count):
            conv = conv + conv_taps[layer, tap][None, :] * padded[tap : tap + gated_in.shape[0]]
        gated = (outer.astype(jnp.float32) * conv).astype(jnp.bfloat16)
        terms = jnp.dot(gated, all_output[layer], preferred_element_type=jnp.float32)
        branch = lax.psum_scatter(
            terms.astype(jnp.bfloat16), "tp", scatter_dimension=1, tiled=True
        ).astype(jnp.float32)
        pre = alpha * state.astype(jnp.float32) + branch
        total, squares = lax.psum(
            (jnp.sum(pre, axis=-1, keepdims=True), jnp.sum(pre * pre, axis=-1, keepdims=True)), "tp"
        )
        mean = total / D
        var = jnp.maximum(squares / D - mean * mean, 0.0)
        normed = (pre - mean) * lax.rsqrt(var + 1e-05)
        state = (normed * norm_gain[layer][None, :] + norm_bias[layer][None, :]).astype(
            jnp.bfloat16
        )
    return state


def solution(mesh):
    in_specs = (
        P("sp", "tp"),
        P(None, "sp", "tp"),
        P(None, "sp", "tp"),
        P(None, "sp", "tp"),
        P(None, None, "tp"),
        P(None, "tp", "sp"),
        P(None, "tp"),
        P(None, "tp"),
    )
    out_specs = P("sp", "tp")
    return jax.shard_map(shards, mesh=mesh, in_specs=in_specs, out_specs=out_specs, check_vma=False)
```

profile of v0, /device:TPU:0, one launch (start us, length us, event | category | flops | bytes accessed | tf_op | source)
XLA Modules:
  0.0 578.4 jit_solution(5210033657117156722)
XLA Ops:
  6.5 0.0 all-gather.7.cloned.1.call-start
  6.5 0.7 all-gather.7.cloned.1.call-update
  7.3 0.0 all-gather.13.cloned.1.call-start
  7.3 0.7 all-gather.13.cloned.1.call-update
  8.0 0.0 all-gather.11.cloned.1.call-start
  8.1 0.7 all-gather.11.cloned.1.call-update
  8.7 0.0 all-gather.15.cloned.1.call-start
  8.8 0.5 all-gather.15.cloned.1.call-update
  9.3 0.0 all-gather.9.cloned.1.call-start
  9.4 0.5 all-gather.9.cloned.1.call-update
  9.9 0.0 copy-start.2
  9.9 0.0 reduce-scatter.3.cloned.1.call-start
  10.0 10.7 %all-gather.7.cloned.1.call-done = bf16[256,2048]{1,0:T(8,128)(2,1)} async-done(((bf16[256,1024]{1,0:T(8,128)(2,1)}), bf16[256,2048]{1,0:T(8,128)(2,1)}) %all-gather.7.cloned.1.call-update) | async-done | bytes 1048592 | tf_op jit(solution)/shard_map/all_gather | solution.py:38
  20.7 116.2 %all-gather.13.cloned.1.call-done = bf16[2,2048,1024]{2,1,0:T(8,128)(2,1)} async-done(((bf16[2,128,1024]{2,1,0:T(8,128)(2,1)}), bf16[2,2048,1024]{2,1,0:T(8,128)(2,1)}) %all-gather.13.cloned.1.call-update) | async-done | bytes 8388624 | tf_op jit(solution)/shard_map/all_gather | solution.py:32
  136.8 4.7 fusion.16
  141.5 108.4 %all-gather.11.cloned.1.call-done = bf16[2,2048,1024]{2,1,0:T(8,128)(2,1)} async-done(((bf16[2,128,1024]{2,1,0:T(8,128)(2,1)}), bf16[2,2048,1024]{2,1,0:T(8,128)(2,1)}) %all-gather.11.cloned.1.call-update) | async-done | bytes 8388624 | tf_op jit(solution)/shard_map/all_gather | solution.py:34
  250.0 0.0 copy-done.5
  250.0 3.8 fusion.14
  253.8 3.4 collective-permute-start
  257.1 0.0 copy-done.2
  257.2 135.4 %all-gather.15.cloned.1.call-done = bf16[2,1024,2048]{2,1,0:T(8,128)(2,1)} async-done(((bf16[2,1024,128]{2,1,0:T(8,128)(2,1)}), bf16[2,1024,2048]{2,1,0:T(8,128)(2,1)}) %all-gather.15.cloned.1.call-update) | async-done | bytes 8388624 | tf_op jit(solution)/shard_map/all_gather | solution.py:35
  392.6 113.0 %all-gather.9.cloned.1.call-done = bf16[2,2048,1024]{2,1,0:T(8,128)(2,1)} async-done(((bf16[2,128,1024]{2,1,0:T(8,128)(2,1)}), bf16[2,2048,1024]{2,1,0:T(8,128)(2,1)}) %all-gather.9.cloned.1.call-update) | async-done | bytes 8388624 | tf_op jit(solution)/shard_map/all_gather | solution.py:33
  505.6 0.0 collective-permute-done
  505.6 7.0 %fusion.8 = bf16[256,2048]{1,0:T(8,128)(2,1)} fusion(bf16[2,1024,2048]{2,1,0:T(8,128)(2,1)} %all-gather.15.cloned.1.call-done, f32[2,1024]{1,0:T(2,128)S(1)} %collective-permute-done, f32[256,1024]{1,0:T(8,128)S(1)} %fusion.14, bf16[256,2048]{1,0:T(8,128)(2,1)S(1)} %copy-done.5, bf16[2,2048,1024]{2,1,0:T(8,128)(2,1)} %all-gather.9.cloned.1.call-done, ...), kind=kOutput, calls=%fused_computation.16 | convolution fusion | flops 2150891520 | bytes 11554816 | tf_op jit(solution)/shard_map/dot_general | solution.py:49
  512.7 0.0 reduce-scatter.3.cloned.1.call-update
  512.7 0.0 all-gather.17.cloned.1.call-start
  512.8 0.0 copy-done.3
  512.8 0.0 copy-done.4
  512.8 6.6 %reduce-scatter.3.cloned.1.call-done = bf16[256,1024]{1,0:T(8,128)(2,1)} async-done(((bf16[256,2048]{1,0:T(8,128)(2,1)}), bf16[256,1024]{1,0:T(8,128)(2,1)}) %reduce-scatter.3.cloned.1.call-update) | async-done | bytes 524304 | tf_op jit(solution)/shard_map/reduce_scatter | solution.py:50
  519.4 0.0 copy-done.1
  519.4 1.4 fusion.38
  520.8 2.5 all-reduce.1
  523.3 2.2 add_convert_fusion.1
  525.5 0.0 all-gather.17.cloned.1.call-update
  525.5 0.0 reduce-scatter.5.cloned.1.call-start
  525.5 10.3 %all-gather.17.cloned.1.call-done = bf16[256,2048]{1,0:T(8,128)(2,1)} async-done(((bf16[256,1024]{1,0:T(8,128)(2,1)}), bf16[256,2048]{1,0:T(8,128)(2,1)}) %all-gather.17.cloned.1.call-update) | async-done | bytes 1048592 | tf_op jit(solution)/shard_map/all_gather | solution.py:38
  535.9 3.8 fusion.23
  539.7 0.0 copy-done.6
  539.7 3.5 fusion.21
  543.2 3.6 collective-permute-start.1
  546.9 1.3 collective-permute-done.1
  548.2 7.0 %fusion.9 = bf16[256,2048]{1,0:T(8,128)(2,1)} fusion(bf16[2,1024,2048]{2,1,0:T(8,128)(2,1)} %all-gather.15.cloned.1.call-done, f32[2,1024]{1,0:T(2,128)S(1)} %collective-permute-done.1, f32[256,1024]{1,0:T(8,128)S(1)} %fusion.21, bf16[256,2048]{1,0:T(8,128)(2,1)S(1)} %copy-done.6, bf16[2,2048,1024]{2,1,0:T(8,128)(2,1)} %all-gather.9.cloned.1.call-done, ...), kind=kOutput, calls=%fused_computation.17 | convolution fusion | flops 2150891520 | bytes 11554816 | tf_op jit(solution)/shard_map/dot_general | solution.py:49
  555.3 0.0 reduce-scatter.5.cloned.1.call-update
  555.3 10.3 %reduce-scatter.5.cloned.1.call-done = bf16[256,1024]{1,0:T(8,128)(2,1)} async-done(((bf16[256,2048]{1,0:T(8,128)(2,1)}), bf16[256,1024]{1,0:T(8,128)(2,1)}) %reduce-scatter.5.cloned.1.call-update) | async-done | bytes 524304 | tf_op jit(solution)/shard_map/reduce_scatter | solution.py:50
  565.5 0.0 copy-done
  565.5 1.4 fusion.39
  566.9 2.5 all-reduce
  569.4 2.2 add_convert_fusion
  (13 shorter events, 0.1 us)
Async XLA Ops:
  6.5 14.1 %all-gather.7.cloned.1.call-start = ((), (), s32[]{:S(2)}) async-start(), calls=%async_computation.2 | async-start | bytes 1572864 | tf_op jit(solution)/shard_map/all_gather | solution.py:38
  7.3 129.6 %all-gather.13.cloned.1.call-start = ((), (), s32[]{:S(2)}) async-start(), calls=%async_computation.5 | async-start | bytes 8912896 | tf_op jit(solution)/shard_map/all_gather | solution.py:32
  8.0 242.0 %all-gather.11.cloned.1.call-start = ((), (), s32[]{:S(2)}) async-start(), calls=%async_computation.4 | async-start | bytes 8912896 | tf_op jit(solution)/shard_map/all_gather | solution.py:34
  8.7 383.9 %all-gather.15.cloned.1.call-start = ((), (), s32[]{:S(2)}) async-start(), calls=%async_computation.6 | async-start | bytes 8912896 | tf_op jit(solution)/shard_map/all_gather | solution.py:35
  9.3 496.3 %all-gather.9.cloned.1.call-start = ((), (), s32[]{:S(2)}) async-start(), calls=%async_computation.3 | async-start | bytes 8912896 | tf_op jit(solution)/shard_map/all_gather | solution.py:33
  9.9 247.2 %copy-start.2 = (f32[2,3,1024]{2,0,1:T(2,128)S(1)}, f32[2,3,1024]{2,0,1:T(2,128)}, u32[]{:S(2)}) copy-start(f32[2,3,1024]{2,0,1:T(2,128)} %param.12) | copy-start | bytes 73732
  9.9 509.5 %reduce-scatter.3.cloned.1.call-start = ((), (), s32[]{:S(2)}) async-start(), calls=%async_computation.7 | async-start | bytes 1572864 | tf_op jit(solution)/shard_map/reduce_scatter | solution.py:50
  20.7 229.3 %copy-start.5 = (bf16[256,2048]{1,0:T(8,128)(2,1)S(1)}, bf16[256,2048]{1,0:T(8,128)(2,1)}, u32[]{:S(2)}) copy-start(bf16[256,2048]{1,0:T(8,128)(2,1)} %all-gather.7.cloned.1.call-done) | copy-start | bytes 3145732
  253.8 251.9 %collective-permute-start = (f32[2,1024]{1,0:T(2,128)S(1)}, f32[2,1024]{1,0:T(2,128)S(1)}, u32[]{:S(2)}, u32[]{:S(2)}) collective-permute-start(f32[2,1024]{1,0:T(2,128)S(1)} %slice.99), channel_id=1, source_target_pairs={{0,2},{2,4},{4,6},{6,8},{8,10},{10,12},{12,14},{14,16},{16,18},{18... | collective-permute-start | bytes 24584 | tf_op jit(solution)/shard_map/ppermute | solution.py:13
  505.6 7.1 %copy-start.3 = (f32[2,1024]{1,0:T(2,128)S(1)}, f32[2,1024]{1,0:T(2,128)}, u32[]{:S(2)}) copy-start(f32[2,1024]{1,0:T(2,128)} %param.14) | copy-start | bytes 24580
  505.6 7.2 %copy-start.4 = (f32[2,1024]{1,0:T(2,128)S(1)}, f32[2,1024]{1,0:T(2,128)}, u32[]{:S(2)}) copy-start(f32[2,1024]{1,0:T(2,128)} %param.15) | copy-start | bytes 24580
  505.6 13.8 %copy-start.1 = (bf16[256,1024]{1,0:T(8,128)(2,1)S(1)}, bf16[256,1024]{1,0:T(8,128)(2,1)}, u32[]{:S(2)}) copy-start(bf16[256,1024]{1,0:T(8,128)(2,1)} %param.8) | copy-start | bytes 1572868
  512.7 23.1 %all-gather.17.cloned.1.call-start = ((), (), s32[]{:S(2)}) async-start(), calls=%async_computation.8 | async-start | bytes 1572864 | tf_op jit(solution)/shard_map/all_gather | solution.py:38
  525.5 40.1 %reduce-scatter.5.cloned.1.call-start = ((), (), s32[]{:S(2)}) async-start(), calls=%async_computation.9 | async-start | bytes 1572864 | tf_op jit(solution)/shard_map/reduce_scatter | solution.py:50
  535.9 3.8 copy-start.6
  543.2 5.0 collective-permute-start.1
  548.2 17.3 %copy-start = (bf16[256,1024]{1,0:T(8,128)(2,1)S(1)}, bf16[256,1024]{1,0:T(8,128)(2,1)}, u32[]{:S(2)}) copy-start(bf16[256,1024]{1,0:T(8,128)(2,1)} %add_convert_fusion.1) | copy-start | bytes 1572868
Sparse Core Ops, SparseCore 0:
  8.9 11.7 all-gather.6
  23.4 113.3 all-gather.12
  139.6 110.3 all-gather.10
  252.6 140.0 all-gather.14
  395.2 110.3 all-gather.8
  512.8 6.5 reduce-scatter.2
  525.6 10.2 all-gather.16
  555.4 10.0 reduce-scatter.4
where the time goes:
time: 579 us; the launch traced here: 578 us
  waiting for transfers between devices  515 us (89%)
  matrix products  29.9 us (5%)
  between operations  13.6 us (2%)
  starting transfers between devices  7.27 us (1%)
  other arithmetic  7.1 us (1%)
    all_gather x1, waiting for transfers between devices, shards(): lax.all_gather(output_weight, 'sp', axis=2, tiled=True)  135 us
    all_gather x1, waiting for transfers between devices, shards(): lax.all_gather(value_weight, 'sp', axis=1, tiled=True)  116 us
    all_gather x1, waiting for transfers between devices, shards(): lax.all_gather(outer_weight, 'sp', axis=1, tiled=True)  113 us
    all_gather x1, waiting for transfers between devices, shards(): lax.all_gather(inner_weight, 'sp', axis=1, tiled=True)  108 us
    all_gather x2, waiting for transfers between devices, shards(): whole = lax.all_gather(state, 'tp', axis=1, tiled=True)  21 us
    reduce_scatter x2, waiting for transfers between devices, shards(): lax.psum_scatter(terms.astype(jnp.bfloat16), 'tp', scatter_dimension=1, t...  16.9 us
    dot_general x4, matrix products, input_products(): jnp.dot(whole, weight, preferred_element_type=jnp.float32)  15.8 us
    dot_general x2, matrix products, shards(): jnp.dot(gated, all_output[layer], preferred_element_type=jnp.float32)  14.1 us
  transfers between devices with their start and end apart: 10, of which 9 were waited for; matrix products, arithmetic and copies ran while one was open for 1% of the time, Pallas kernels for 0%

commit v1 on v0

v1 whole, which is shorter than its diff:
```python
import jax
import jax.numpy as jnp
from jax import lax
from jax.experimental import pallas as pl
from jax.experimental.pallas import tpu as pltpu
from jax.sharding import PartitionSpec as P

LANES = 128
EPS = 1e-5


def flip(j, i):
    if i & 1:
        j = j + 1 - 2 * lax.rem(j, 2)
    if i & 2:
        j = j + 2 - 4 * lax.rem(lax.div(j, 2), 2)
    return j


def plane_size(sp, channels):
    q = 4
    while q > 1 and (sp % q or channels // q < LANES or channels % q):
        q //= 2
    return q


def make_kernel(sp, tp, q, layers, taps_count, rows, feats, depth, width, alpha):
    line = sp // q
    units = layers * 4
    model = feats * tp
    per_half = sp // tp

    def kernel(
        tok, val, outw, inn, taps, prj, gain, bias, res,
        xg, win, wout, state, ubuf, obuf, zpad, gated, part, rec1, snd2, rec2, acc, stat, stat_in, halo,
        a_send, a_recv, a_loc, u_send, u_recv, d_send, d_recv,
        g_send, g_recv, g_loc, t_send, t_recv, p_send, p_recv, r_send, r_recv, s_send, s_recv, h_send, h_recv,
    ):
        me = lax.axis_index("sp")
        c = lax.axis_index("tp")
        l = lax.div(me, q)
        j = lax.rem(me, q)

        def at_sp(other):
            return {"sp": other, "tp": c}

        def at_tp(r):
            return {"sp": me, "tp": lax.rem(c + r, tp)}

        def remote(src, dst, ssem, rsem, dev):
            return pltpu.make_async_remote_copy(
                src_ref=src, dst_ref=dst, send_sem=ssem, recv_sem=rsem,
                device_id=dev, device_id_type=pl.DeviceIdType.MESH,
            )

        def peer(i):
            return l * q + flip(j, i)

        barrier = pltpu.get_barrier_semaphore()

        def greet(dev):
            pl.semaphore_signal(barrier, inc=1, device_id=dev, device_id_type=pl.DeviceIdType.MESH)

        for i in range(1, q):
            greet(at_sp(peer(i)))
        for r in range(1, tp):
            greet(at_tp(r))

        @pl.when(l > 0)
        def _():
            greet(at_sp(me - q))

        @pl.when(l < line - 1)
        def _():
            greet(at_sp(me + q))

        neighbours = (l > 0).astype(jnp.int32) + (l < line - 1).astype(jnp.int32)
        pl.semaphore_wait(barrier, (q - 1) + (tp - 1) + neighbours)

        ORDER = (val, inn, outw, prj)

        def own_piece(k, jd):
            layer, w = divmod(k, 4)
            at = pl.ds(pl.multiple_of(jd * width, width), width)
            if w == 3:
                return prj.at[layer, at, :]
            return ORDER[w].at[layer, :, at]

        def landed(k, s):
            layer, w = divmod(k, 4)
            if w == 3:
                return wout.at[layer, s]
            return win.at[layer, w, pl.ds(pl.multiple_of(s * depth, depth), depth), :]

        def block(k, b):
            layer, w = divmod(k, 4)
            if w == 3:
                return wout.at[layer, pl.ds(b * q, q)]
            return win.at[layer, w, pl.ds(pl.multiple_of(b * (q * depth), q * depth), q * depth), :]

        def a_copy(k, i):
            return remote(own_piece(k, flip(j, i)), landed(k, me), a_send.at[k, i], a_recv.at[k, i], at_sp(peer(i)))

        def a_local(k):
            return pltpu.make_async_copy(own_piece(k, j), landed(k, me), a_loc.at[k])

        def scatter_start(k):
            a_local(k).start()
            for i in range(q - 1, 0, -1):
                a_copy(k, i).start()

        def scatter_wait(k):
            a_local(k).wait()
            for i in range(q - 1, 0, -1):
                a_copy(k, i).wait()

        def up(k, s):
            return remote(block(k, l - s), block(k, l - s), u_send.at[k, s], u_recv.at[k, s], at_sp(me + q))

        def down(k, s):
            return remote(block(k, l + s), block(k, l + s), d_send.at[k, s], d_recv.at[k, s], at_sp(me - q))

        def line_start(k, s):
            @pl.when((l - s >= 0) & (l < line - 1))
            def _():
                up(k, s).start()

            @pl.when((l + s < line) & (l > 0))
            def _():
                down(k, s).start()

        def line_recv(k, s):
            @pl.when(l - 1 - s >= 0)
            def _():
                up(k, s).wait_recv()

            @pl.when(l + 1 + s < line)
            def _():
                down(k, s).wait_recv()

        def line_sent(k, s):
            @pl.when((l - s >= 0) & (l < line - 1))
            def _():
                up(k, s).wait_send()

            @pl.when((l + s < line) & (l > 0))
            def _():
                down(k, s).wait_send()

        def src_of(layer):
            return tok if layer == 0 else state.at[layer - 1]

        def spot(layer, jj):
            return xg.at[layer, c, pl.ds(pl.multiple_of(jj * rows, rows), rows), :]

        def g_copy(layer, i):
            return remote(src_of(layer), spot(layer, j), g_send.at[layer, i], g_recv.at[layer, i], at_sp(peer(i)))

        def g_local(layer):
            return pltpu.make_async_copy(src_of(layer), spot(layer, j), g_loc.at[layer])

        def t_copy(layer, r, i):
            jj = flip(j, i)
            src = src_of(layer) if i == 0 else spot(layer, jj)
            return remote(src, spot(layer, jj), t_send.at[layer, r, i], t_recv.at[layer, r, i], at_tp(r))

        def gather_start(layer):
            g_local(layer).start()
            for i in range(q - 1, 0, -1):
                g_copy(layer, i).start()
            for r in range(1, tp):
                t_copy(layer, r, 0).start()

        def gather_forward(layer):
            for i in range(1, q):
                g_copy(layer, i).wait()
                for r in range(1, tp):
                    t_copy(layer, r, i).start()

        def gather_wait(layer):
            g_local(layer).wait()
            for i in range(q):
                for r in range(1, tp):
                    t_copy(layer, r, i).wait()

        def project(layer, w, store):
            def tile(i, carry):
                at = pl.ds(pl.multiple_of(i * rows, rows), rows)
                total = jnp.zeros((rows, width), jnp.float32)
                for cc in range(tp):
                    total = total + jnp.dot(
                        xg[layer, cc, at, :],
                        win[layer, w, pl.ds(cc * feats, feats), :],
                        preferred_element_type=jnp.float32,
                    )
                store(i, total.astype(jnp.bfloat16))
                return carry

            lax.fori_loop(0, q, tile, 0)

        def put_u(i, v):
            ubuf[pl.ds(pl.multiple_of(i * rows, rows), rows), :] = v

        def put_o(i, v):
            obuf[pl.ds(pl.multiple_of(i * rows, rows), rows), :] = v

        def put_z(i, v):
            at = pl.ds(pl.multiple_of(i * rows, rows), rows)
            zpad[pl.ds(pl.multiple_of(8 + i * rows, 8), rows), :] = v.astype(jnp.float32) * ubuf[at, :].astype(jnp.float32)

        def h_copy(layer):
            return remote(
                halo.at[layer, 0], halo.at[layer, 1], h_send.at[layer], h_recv.at[layer], at_sp(me + q)
            )

        def halo_start(layer):
            halo[layer, 0] = zpad[pl.ds(q * rows, 8), :]

            @pl.when(l < line - 1)
            def _():
                h_copy(layer).start()

        def halo_wait(layer):
            zpad[0:8, :] = jnp.zeros((8, width), jnp.float32)

            @pl.when(l > 0)
            def _():
                h_copy(layer).wait_recv()
                zpad[0:8, :] = halo[layer, 1]

            @pl.when(l < line - 1)
            def _():
                h_copy(layer).wait_send()

        def convolve(layer):
            at_c = pl.ds(pl.multiple_of(j * width, width), width)
            rates = [taps[layer, pl.ds(k, 1), at_c] for k in range(taps_count)]
            for i in range(q):
                conv = jnp.zeros((rows, width), jnp.float32)
                for k in range(taps_count):
                    first = 8 - (taps_count - 1) + k + i * rows
                    conv = conv + rates[k] * zpad[first:first + rows, :]
                at = pl.ds(i * rows, rows)
                gated[at, :] = (obuf[at, :].astype(jnp.float32) * conv).astype(jnp.bfloat16)

        def tile_at(jj):
            return pl.ds(pl.multiple_of(jj * rows, rows), rows)

        def p_copy(layer, r, i):
            at = tile_at(flip(j, i))
            return remote(
                part.at[layer, lax.rem(c + r, tp), at, :], rec1.at[layer, r - 1, at, :],
                p_send.at[layer, r, i], p_recv.at[layer, r, i], at_tp(r),
            )

        def out_product(layer):
            for i in range(q - 1, -1, -1):
                at = tile_at(flip(j, i))

                def half(cc, carry):
                    weight = jnp.concatenate([wout[layer, cc * per_half + b] for b in range(per_half)], axis=1)
                    part[layer, cc, at, :] = jnp.dot(
                        gated[at, :], weight, preferred_element_type=jnp.float32
                    ).astype(jnp.bfloat16)
                    return carry

                lax.fori_loop(0, tp, half, 0)
                for r in range(1, tp):
                    p_copy(layer, r, i).start()

        def r_copy(layer, i):
            return remote(snd2.at[layer, i], rec2.at[layer, i], r_send.at[layer, i], r_recv.at[layer, i], at_sp(peer(i)))

        def reduce_start(layer):
            for i in range(q - 1, -1, -1):
                at = tile_at(flip(j, i))
                total = part[layer, c, at, :].astype(jnp.float32)
                for r in range(1, tp):
                    p_copy(layer, r, i).wait()
                    total = total + rec1[layer, r - 1, at, :].astype(jnp.float32)
                if i:
                    snd2[layer, i] = total.astype(jnp.bfloat16)
                    r_copy(layer, i).start()
                else:
                    acc[...] = total

        def s_copy(layer, r):
            return remote(stat.at[layer], stat_in.at[layer, r], s_send.at[layer, r], s_recv.at[layer, r], at_tp(r))

        def finish(layer):
            pre = alpha * src_of(layer)[...].astype(jnp.float32) + acc[...]
            for i in range(1, q):
                r_copy(layer, i).wait()
                pre = pre + rec2[layer, i].astype(jnp.float32)
            acc[...] = pre
            mine = jnp.sum(pre, axis=-1, keepdims=True)
            away = pre - mine * (1.0 / feats)
            spread = jnp.sum(away * away, axis=-1, keepdims=True)
            lane = lax.broadcasted_iota(jnp.int32, (rows, LANES), 1)
            stat[layer] = jnp.where(lane == 0, mine, spread)
            for r in range(1, tp):
                s_copy(layer, r).start()
            sums, spreads = [mine], [spread]
            for r in range(1, tp):
                s_copy(layer, r).wait()
                sums.append(stat_in[layer, r, :, 0:1])
                spreads.append(stat_in[layer, r, :, 1:2])
            mean = sum(sums[1:], sums[0]) * (1.0 / model)
            var = sum(spreads[1:], spreads[0])
            for s in sums:
                off = s * (1.0 / feats) - mean
                var = var + feats * off * off
            scale = lax.rsqrt(var * (1.0 / model) + EPS)
            normed = (acc[...] - mean) * scale
            y = (normed * gain[pl.ds(layer, 1), :] + bias[pl.ds(layer, 1), :]).astype(jnp.bfloat16)
            if layer == layers - 1:
                res[...] = y
            else:
                state[layer] = y

        for k in range(min(2, units)):
            scatter_start(k)
        gather_start(0)
        for k in range(2, units):
            scatter_start(k)

        def ready(k):
            layer, w = divmod(k, 4)
            if w == 0:
                if layer == 0:
                    gather_wait(0)
                    project(0, 0, put_u)
            elif layer == 0:
                if w == 1:
                    project(0, 1, put_z)
                    halo_start(0)
                elif w == 2:
                    project(0, 2, put_o)
                    halo_wait(0)
                    convolve(0)
                else:
                    out_product(0)

        def layer_rest(layer):
            gather_forward(layer)
            gather_wait(layer)
            project(layer, 0, put_u)
            project(layer, 1, put_z)
            halo_start(layer)
            project(layer, 2, put_o)
            halo_wait(layer)
            convolve(layer)
            out_product(layer)
            reduce_start(layer)
            finish(layer)

        steps = line - 1
        for t in range(units + steps):
            if t < units:
                scatter_wait(t)
                line_start(t, 0)
            for s in range(1, steps):
                if 0 <= t - s < units:
                    line_recv(t - s, s - 1)
                    line_start(t - s, s)
            if t == 1:
                gather_forward(0)
            k = t - steps
            if 0 <= k < units:
                line_recv(k, steps - 1)
                ready(k)
                if k == 4:
                    reduce_start(0)
                if k == 5:
                    finish(0)
                    if layers > 1:
                        gather_start(1)
        for layer in range(1, layers):
            if layer > 1:
                gather_start(layer)
            layer_rest(layer)
        for k in range(units):
            for s in range(steps):
                line_sent(k, s)

    return kernel


def solution(mesh):
    sp, tp = mesh.shape["sp"], mesh.shape["tp"]

    def shards(tokens, value_weight, outer_weight, inner_weight, conv_taps, output_weight, norm_gain, norm_bias):
        rows, feats = tokens.shape
        layers, depth, channels = value_weight.shape
        taps_count = conv_taps.shape[1]
        q = plane_size(sp, channels)
        width = channels // q
        line = sp // q
        model = feats * tp
        alpha = (2.0 * layers) ** 0.25
        out_cols = output_weight.shape[2]
        bf, f32 = jnp.bfloat16, jnp.float32
        kernel = make_kernel(sp, tp, q, layers, taps_count, rows, feats, depth, width, alpha)
        dma = pltpu.SemaphoreType.DMA
        units, steps = 4 * layers, max(line - 1, 1)
        others = max(tp - 1, 1)
        vm = pl.BlockSpec(memory_space=pltpu.VMEM)
        return pl.pallas_call(
            kernel,
            out_shape=jax.ShapeDtypeStruct((rows, feats), bf),
            in_specs=[vm] * 8,
            out_specs=vm,
            scratch_shapes=[
                pltpu.VMEM((layers, tp, q * rows, feats), bf),
                pltpu.VMEM((layers, 3, model, width), bf),
                pltpu.VMEM((layers, sp, width, out_cols), bf),
                pltpu.VMEM((layers, rows, feats), bf),
                pltpu.VMEM((q * rows, width), bf),
                pltpu.VMEM((q * rows, width), bf),
                pltpu.VMEM((q * rows + 8, width), f32),
                pltpu.VMEM((q * rows, width), bf),
                pltpu.VMEM((layers, tp, q * rows, feats), bf),
                pltpu.VMEM((layers, others, q * rows, feats), bf),
                pltpu.VMEM((layers, q, rows, feats), bf),
                pltpu.VMEM((layers, q, rows, feats), bf),
                pltpu.VMEM((rows, feats), f32),
                pltpu.VMEM((layers, rows, LANES), f32),
                pltpu.VMEM((layers, tp, rows, LANES), f32),
                pltpu.VMEM((layers, 2, 8, width), f32),
                dma((units, q)), dma((units, q)), dma((units,)),
                dma((units, steps)), dma((units, steps)), dma((units, steps)), dma((units, steps)),
                dma((layers, q)), dma((layers, q)), dma((layers,)),
                dma((layers, tp, q)), dma((layers, tp, q)),
                dma((layers, tp, q)), dma((layers, tp, q)),
                dma((layers, q)), dma((layers, q)),
                dma((layers, tp)), dma((layers, tp)),
                dma((layers,)), dma((layers,)),
            ],
            compiler_params=pltpu.CompilerParams(
                collective_id=0, has_side_effects=True, vmem_limit_bytes=60 * 1024 * 1024
            ),
        )(tokens, value_weight, outer_weight, inner_weight, conv_taps, output_weight, norm_gain, norm_bias)

    in_specs = (
        P("sp", "tp"),
        P(None, "sp", "tp"),
        P(None, "sp", "tp"),
        P(None, "sp", "tp"),
        P(None, None, "tp"),
        P(None, "tp", "sp"),
        P(None, "tp"),
        P(None, "tp"),
    )
    return jax.shard_map(shards, mesh=mesh, in_specs=in_specs, out_specs=P("sp", "tp"), check_vma=False)
```

time: 579 us -> 220 us (0.38)
  waiting for transfers between devices: 515 us -> 0 us
  Pallas kernels: 0 us -> 216 us
  matrix products: 29.9 us -> 0 us
  between operations: 13.6 us -> 0.01 us
  starting transfers between devices: 7.27 us -> 0 us
  other arithmetic: 7.1 us -> 0 us
    all_gather x6 -> x0, waiting for transfers between devices: 494 us -> none  [the longest x1 135 us: shards(): lax.all_gather(output_weight, 'sp', axis=2, tiled=True)]
    pallas_call x0 -> x1, Pallas kernels: none -> 216 us  [shards(): pl.pallas_call(kernel, out_shape=jax.ShapeDtypeStruct((rows, feats), bf),...]
    dot_general x6 -> x0, matrix products: 29.9 us -> none  [the longest x4 15.8 us: input_products(): jnp.dot(whole, weight, preferred_element_type=jnp.float32)]
    reduce_scatter x2 -> x0, waiting for transfers between devices: 16.9 us -> none  [shards(): lax.psum_scatter(terms.astype(jnp.bfloat16), 'tp', scatter_dimension=1, t...]
    ppermute x2 -> x0, starting transfers between devices: 6.99 us -> none  [from_behind(): return lax.ppermute(array, axis, pairs)]
  transfers between devices with their start and end apart: 10 -> 0, of which waited for: 9 -> 0; matrix products, arithmetic and copies ran while one was open for 1% -> 0% of each run, Pallas kernels for 0% -> 0%
where the time goes in v1:
time: 220 us
  Pallas kernels  216 us (98%)
  local copies, waits for them, and re-layouts  3.23 us (1%)
    pallas_call x1, Pallas kernels, shards(): pl.pallas_call(kernel, out_shape=jax.ShapeDtypeStruct((rows, feats), bf),...  216 us

profile of v1, /device:TPU:0, one launch (start us, length us, event | category | flops | bytes accessed | tf_op | source)
XLA Modules:
  0.0 219.6 jit_solution(5573817433860513668)
XLA Ops:
  0.0 1.4 copy.9.taps
  1.4 216.4 %shard_map.82 = bf16[256,1024]{1,0:T(8,128)(2,1)} custom-call(bf16[256,1024]{1,0:T(8,128)(2,1)} %tok.1, bf16[2,128,1024]{2,1,0:T(8,128)(2,1)} %val.1, bf16[2,128,1024]{2,1,0:T(8,128)(2,1)} %outw.1, bf16[2,128,1024]{2,1,0:T(8,128)(2,1)} %inn.1, f32[2,3,1024]{2,1,0:T(4,128)} %copy.9.taps, bf16[2,1024,128]{2,1,0:T(8,128)(2,1)} %prj.1, f32[2,1024]{1,0:T(2,128)} %gain.1, ...), custom_call_target="tpu_custom_call" | custom-call | tf_op jit(solution)/shard_map/pallas_call | solution.py:408
  217.8 1.9 copy.11

commit v2 on v1

--- a/solution.py
+++ b/solution.py
@@ -253,11 +253,27 @@
                 p_send.at[layer, r, i], p_recv.at[layer, r, i], at_tp(r),
             )
 
+        def r_copy(layer, i):
+            return remote(snd2.at[layer, i], rec2.at[layer, i], r_send.at[layer, i], r_recv.at[layer, i], at_sp(peer(i)))
+
+        def reduce_tile(layer, i):
+            at = tile_at(flip(j, i))
+            total = part[layer, c, at, :].astype(jnp.float32)
+            for r in range(1, tp):
+                p_copy(layer, r, i).wait()
+                total = total + rec1[layer, r - 1, at, :].astype(jnp.float32)
+            if i:
+                snd2[layer, i] = total.astype(jnp.bfloat16)
+                r_copy(layer, i).start()
+            else:
+                acc[...] = total
+
         def out_product(layer):
             for i in range(q - 1, -1, -1):
                 at = tile_at(flip(j, i))
 
-                def half(cc, carry):
+                def half(n, carry):
+                    cc = lax.rem(c + 1 + n, tp)
                     weight = jnp.concatenate([wout[layer, cc * per_half + b] for b in range(per_half)], axis=1)
                     part[layer, cc, at, :] = jnp.dot(
                         gated[at, :], weight, preferred_element_type=jnp.float32
@@ -267,22 +283,9 @@
                 lax.fori_loop(0, tp, half, 0)
                 for r in range(1, tp):
                     p_copy(layer, r, i).start()
-
-        def r_copy(layer, i):
-            return remote(snd2.at[layer, i], rec2.at[layer, i], r_send.at[layer, i], r_recv.at[layer, i], at_sp(peer(i)))
-
-        def reduce_start(layer):
-            for i in range(q - 1, -1, -1):
-                at = tile_at(flip(j, i))
-                total = part[layer, c, at, :].astype(jnp.float32)
-                for r in range(1, tp):
-                    p_copy(layer, r, i).wait()
-                    total = total + rec1[layer, r - 1, at, :].astype(jnp.float32)
-                if i:
-                    snd2[layer, i] = total.astype(jnp.bfloat16)
-                    r_copy(layer, i).start()
-                else:
-                    acc[...] = total
+                if i < q - 1:
+                    reduce_tile(layer, i + 1)
+            reduce_tile(layer, 0)
 
         def s_copy(layer, r):
             return remote(stat.at[layer], stat_in.at[layer, r], s_send.at[layer, r], s_recv.at[layer, r], at_tp(r))
@@ -324,61 +327,65 @@
         for k in range(2, units):
             scatter_start(k)
 
-        def ready(k):
-            layer, w = divmod(k, 4)
-            if w == 0:
-                if layer == 0:
-                    gather_wait(0)
-                    project(0, 0, put_u)
-            elif layer == 0:
-                if w == 1:
-                    project(0, 1, put_z)
-                    halo_start(0)
-                elif w == 2:
-                    project(0, 2, put_o)
-                    halo_wait(0)
-                    convolve(0)
-                else:
-                    out_product(0)
-
-        def layer_rest(layer):
-            gather_forward(layer)
+        def inputs_of(layer):
             gather_wait(layer)
             project(layer, 0, put_u)
+
+        def middle_of(layer):
             project(layer, 1, put_z)
             halo_start(layer)
+
+        def gates_of(layer):
             project(layer, 2, put_o)
             halo_wait(layer)
             convolve(layer)
+
+        steps = line - 1
+        begin = [k + k // 4 for k in range(units)]
+        for t in range(begin[-1] + steps + 1):
+            for k in range(units):
+                if begin[k] == t:
+                    scatter_wait(k)
+                    line_start(k, 0)
+            for k in range(units):
+                s = t - begin[k]
+                if 1 <= s < steps:
+                    line_recv(k, s - 1)
+                    line_start(k, s)
+            for k in range(units):
+                if t - begin[k] == steps:
+                    line_recv(k, steps - 1)
+            if t == begin[0] + steps - 1:
+                gather_forward(0)
+            if t == begin[0] + steps:
+                inputs_of(0)
+            if t == begin[1] + steps:
+                middle_of(0)
+            if t == begin[2] + steps:
+                gates_of(0)
+            if t == begin[3] + steps:
+                out_product(0)
+            if layers > 1:
+                if t == begin[3] + steps + 1:
+                    finish(0)
+                    gather_start(1)
+                if t == begin[3] + steps + 3:
+                    gather_forward(1)
+                if t == begin[3] + steps + 4:
+                    inputs_of(1)
+                    middle_of(1)
+                    gates_of(1)
+        if layers > 1:
+            out_product(1)
+            finish(1)
+        for layer in range(2, layers):
+            gather_start(layer)
+            gather_forward(layer)
+            inputs_of(layer)
+            middle_of(layer)
+            gates_of(layer)
             out_product(layer)
-            reduce_start(layer)
             finish(layer)
-
-        steps = line - 1
-        for t in range(units + steps):
-            if t < units:
-                scatter_wait(t)
-                line_start(t, 0)
-            for s in range(1, steps):
-                if 0 <= t - s < units:
-                    line_recv(t - s, s - 1)
-                    line_start(t - s, s)
-            if t == 1:
-                gather_forward(0)
-            k = t - steps
-            if 0 <= k < units:
-                line_recv(k, steps - 1)
-                ready(k)
-                if k == 4:
-                    reduce_start(0)
-                if k == 5:
-                    finish(0)
-                    if layers > 1:
-                        gather_start(1)
-        for layer in range(1, layers):
-            if layer > 1:
-                gather_start(layer)
-            layer_rest(layer)
         for k in range(units):
             for s in range(steps):
                 line_sent(k, s)

time: 220 us -> 197 us (0.90)
  Pallas kernels: 216 us -> 194 us
    pallas_call x1, Pallas kernels: 216 us -> 194 us  [shards(): pl.pallas_call(kernel, out_shape=jax.ShapeDtypeStruct((rows, feats), bf),...]
where the time goes in v2:
time: 197 us
  Pallas kernels  194 us (98%)
  local copies, waits for them, and re-layouts  3.23 us (2%)
    pallas_call x1, Pallas kernels, shards(): pl.pallas_call(kernel, out_shape=jax.ShapeDtypeStruct((rows, feats), bf),...  194 us

profile of v2, /device:TPU:0, one launch (start us, length us, event | category | flops | bytes accessed | tf_op | source)
XLA Modules:
  0.0 197.0 jit_solution(11117070636569805333)
XLA Ops:
  0.0 1.4 copy.9.taps
  1.4 193.8 %shard_map.82 = bf16[256,1024]{1,0:T(8,128)(2,1)} custom-call(bf16[256,1024]{1,0:T(8,128)(2,1)} %tok.1, bf16[2,128,1024]{2,1,0:T(8,128)(2,1)} %val.1, bf16[2,128,1024]{2,1,0:T(8,128)(2,1)} %outw.1, bf16[2,128,1024]{2,1,0:T(8,128)(2,1)} %inn.1, f32[2,3,1024]{2,1,0:T(4,128)} %copy.9.taps, bf16[2,1024,128]{2,1,0:T(8,128)(2,1)} %prj.1, f32[2,1024]{1,0:T(2,128)} %gain.1, ...), custom_call_target="tpu_custom_call" | custom-call | tf_op jit(solution)/shard_map/pallas_call | solution.py:415
  195.1 1.9 copy.11

commit v3 on v2

--- a/solution.py
+++ b/solution.py
@@ -253,8 +253,25 @@
                 p_send.at[layer, r, i], p_recv.at[layer, r, i], at_tp(r),
             )
 
-        def r_copy(layer, i):
-            return remote(snd2.at[layer, i], rec2.at[layer, i], r_send.at[layer, i], r_recv.at[layer, i], at_sp(peer(i)))
+        halves = 2 if q == 4 else 1
+        part_rows = rows // halves
+
+        def rows_of(h):
+            return pl.ds(h * part_rows, part_rows)
+
+        def r_copy(layer, i, h):
+            at = rows_of(h)
+            return remote(
+                snd2.at[layer, i, at, :], rec2.at[layer, i, at, :],
+                r_send.at[layer, i, h], r_recv.at[layer, i, h], at_sp(peer(i)),
+            )
+
+        def v_copy(layer, h):
+            at = rows_of(h)
+            return remote(
+                snd2.at[layer, 3, at, :], rec2.at[layer, 3, at, :],
+                r_send.at[layer, 3, h], r_recv.at[layer, 3, h], at_sp(peer(1 + h)),
+            )
 
         def reduce_tile(layer, i):
             at = tile_at(flip(j, i))
@@ -262,11 +279,27 @@
             for r in range(1, tp):
                 p_copy(layer, r, i).wait()
                 total = total + rec1[layer, r - 1, at, :].astype(jnp.float32)
-            if i:
-                snd2[layer, i] = total.astype(jnp.bfloat16)
-                r_copy(layer, i).start()
+            if i == 0:
+                acc[...] = total
+                return
+            snd2[layer, i] = total.astype(jnp.bfloat16)
+            if i == 3:
+                for h in range(2):
+                    v_copy(layer, h).start()
+            elif halves == 2:
+                r_copy(layer, i, i - 1).start()
             else:
-                acc[...] = total
+                r_copy(layer, i, 0).start()
+
+        def relay(layer):
+            if halves == 2:
+                for h in range(2):
+                    v_copy(layer, h).wait()
+                    i, at = 2 - h, rows_of(h)
+                    snd2[layer, i, at, :] = (
+                        snd2[layer, i, at, :].astype(jnp.float32) + rec2[layer, 3, at, :].astype(jnp.float32)
+                    ).astype(jnp.bfloat16)
+                    r_copy(layer, i, h).start()
 
         def out_product(layer):
             for i in range(q - 1, -1, -1):
@@ -286,14 +319,16 @@
                 if i < q - 1:
                     reduce_tile(layer, i + 1)
             reduce_tile(layer, 0)
+            relay(layer)
 
         def s_copy(layer, r):
             return remote(stat.at[layer], stat_in.at[layer, r], s_send.at[layer, r], s_recv.at[layer, r], at_tp(r))
 
         def finish(layer):
             pre = alpha * src_of(layer)[...].astype(jnp.float32) + acc[...]
-            for i in range(1, q):
-                r_copy(layer, i).wait()
+            for i in range(1, min(q, 3)):
+                for h in range(halves):
+                    r_copy(layer, i, h).wait()
                 pre = pre + rec2[layer, i].astype(jnp.float32)
             acc[...] = pre
             mine = jnp.sum(pre, axis=-1, keepdims=True)
@@ -439,7 +474,7 @@
                 dma((layers, q)), dma((layers, q)), dma((layers,)),
                 dma((layers, tp, q)), dma((layers, tp, q)),
                 dma((layers, tp, q)), dma((layers, tp, q)),
-                dma((layers, q)), dma((layers, q)),
+                dma((layers, q, 2)), dma((layers, q, 2)),
                 dma((layers, tp)), dma((layers, tp)),
                 dma((layers,)), dma((layers,)),
             ],

time: 197 us -> 191 us (0.970)
  Pallas kernels: 194 us -> 187 us
    pallas_call x1, Pallas kernels: 194 us -> 187 us  [shards(): pl.pallas_call(kernel, out_shape=jax.ShapeDtypeStruct((rows, feats), bf),...]
where the time goes in v3:
time: 191 us; the launch traced here: 190 us
  Pallas kernels  187 us (98%)
  local copies, waits for them, and re-layouts  3.23 us (2%)
    pallas_call x1, Pallas kernels, shards(): pl.pallas_call(kernel, out_shape=jax.ShapeDtypeStruct((rows, feats), bf),...  187 us

profile of v3, /device:TPU:0, one launch (start us, length us, event | category | flops | bytes accessed | tf_op | source)
XLA Modules:
  0.0 190.3 jit_solution(10359917954718293049)
XLA Ops:
  0.0 1.4 copy.9.taps
  1.4 187.0 %shard_map.82 = bf16[256,1024]{1,0:T(8,128)(2,1)} custom-call(bf16[256,1024]{1,0:T(8,128)(2,1)} %tok.1, bf16[2,128,1024]{2,1,0:T(8,128)(2,1)} %val.1, bf16[2,128,1024]{2,1,0:T(8,128)(2,1)} %outw.1, bf16[2,128,1024]{2,1,0:T(8,128)(2,1)} %inn.1, f32[2,3,1024]{2,1,0:T(4,128)} %copy.9.taps, bf16[2,1024,128]{2,1,0:T(8,128)(2,1)} %prj.1, f32[2,1024]{1,0:T(2,128)} %gain.1, ...), custom_call_target="tpu_custom_call" | custom-call | tf_op jit(solution)/shard_map/pallas_call | solution.py:450
  188.4 1.9 copy.11
